TPU v7x, 32 devices: a whole 2x2x4 slice. The times are simulated.
32 devices in a mesh: sp: 8 (over z, x), tp: 4 (over y, core).
Axes of the slice: x: 2, y: 2, z: 4, core: 2. Of those that a mesh axis runs over, the one named last changes fastest.
Arguments:
- stream: bfloat16 [4096, 2048], P('sp', 'tp'), may hold values from -6 to 6
- norm_gain: float32 [2, 2048], replicated, may hold values from 0.1 to 1.9
- w_value: bfloat16 [2, 2048, 2048], P(None, 'sp', 'tp'), may hold values from -0.125 to 0.125
- w_inner: bfloat16 [2, 2048, 2048], P(None, 'sp', 'tp'), may hold values from -0.125 to 0.125
- w_outer: bfloat16 [2, 2048, 2048], P(None, 'sp', 'tp'), may hold values from -0.125 to 0.125
- conv_taps: float32 [2, 3, 2048], P(None, None, 'tp'), may hold values from -3 to 3
- w_output: bfloat16 [2, 2048, 2048], P(None, 'tp', 'sp'), may hold values from -0.125 to 0.125
Outputs:
- result: bfloat16 [4096, 2048], P('sp', 'tp')
All inputs are finite; a program needn't handle non-finite values.
Results may differ from a plain program's by a relative error of at most 0.02.
Values may be sent and summed in bfloat16 or wider, within the bound.
A program may use at most 64 MiB of HBM per device.

v0:
```python
import jax
import jax.numpy as jnp
from jax import lax
from jax.sharding import PartitionSpec as P

LAYERS = 2
EPSILON = 1e-06


def passed_along(block, axis, distance):
    devices = range(lax.axis_size(axis))
    route = [(i - distance, i) for i in devices if i - distance in devices]
    return lax.ppermute(block, axis, route)


def on_device(stream, norm_gain, w_value, w_inner, w_outer, conv_taps, w_output):
    gathered_in = (
        lax.all_gather(w_value, "sp", axis=1, tiled=True),
        lax.all_gather(w_inner, "sp", axis=1, tiled=True),
        lax.all_gather(w_outer, "sp", axis=1, tiled=True),
    )
    gathered_out = lax.all_gather(w_output, "sp", axis=2, tiled=True)
    stream_now = stream
    for layer_index in range(LAYERS):
        layer_value = gathered_in[0][layer_index]
        layer_inner = gathered_in[1][layer_index]
        layer_outer = gathered_in[2][layer_index]
        layer_output = gathered_out[layer_index]
        full_rows = lax.all_gather(stream_now, "tp", axis=1, tiled=True)
        row_float = full_rows.astype(jnp.float32)
        scale = lax.rsqrt(jnp.mean(row_float * row_float, axis=-1, keepdims=True) + EPSILON)
        normed = (row_float * scale * norm_gain[layer_index]).astype(jnp.bfloat16)
        row_count = normed.shape[0]
        value_proj = jnp.dot(normed, layer_value, preferred_element_type=jnp.float32)
        inner_gate = jnp.dot(normed, layer_inner, preferred_element_type=jnp.float32)
        outer_gate = jnp.dot(normed, layer_outer, preferred_element_type=jnp.float32)
        mixed = (inner_gate * value_proj).astype(jnp.bfloat16)
        before = passed_along(mixed[row_count - 2 :], "sp", 1)
        padded = jnp.concatenate([before, mixed], axis=0).astype(jnp.float32)
        taps = conv_taps[layer_index]
        convolved = (
            taps[0] * padded[0:row_count]
            + taps[1] * padded[1 : row_count + 1]
            + taps[2] * padded[2:]
        )
        gated = (outer_gate * convolved).astype(jnp.bfloat16)
        terms = jnp.dot(gated, layer_output, preferred_element_type=jnp.float32).astype(
            jnp.bfloat16
        )
        summed = lax.psum_scatter(
            terms.astype(jnp.float32).astype(jnp.bfloat16), "tp", scatter_dimension=1, tiled=True
        ).astype(jnp.float32)
        stream_now = (stream_now.astype(jnp.float32) + summed).astype(jnp.bfloat16)
    return stream_now


def solution(mesh):
    in_specs = (
        P("sp", "tp"),
        P(),
        P(None, "sp", "tp"),
        P(None, "sp", "tp"),
        P(None, "sp", "tp"),
        P(None, None, "tp"),
        P(None, "tp", "sp"),
    )
    out_specs = P("sp", "tp")
    return jax.shard_map(
        on_device, mesh=mesh, in_specs=in_specs, out_specs=out_specs, check_vma=False
    )
```

profile of v0, /device:TPU:0, one launch (start us, length us, event | category | flops | bytes accessed | tf_op | source)
XLA Modules:
  0.0 450.2 jit_solution(300876081806969072)
XLA Ops:
  6.5 0.7 all-gather.7.cloned.1.call-update
  7.3 0.7 all-gather.13.cloned.1.call-update
  10.0 24.2 %all-gather.7.cloned.1.call-done = bf16[512,2048]{1,0:T(8,128)(2,1)} async-done(((bf16[512,512]{1,0:T(8,128)(2,1)}), bf16[512,2048]{1,0:T(8,128)(2,1)}) %all-gather.7.cloned.1.call-update) | async-done | bytes 2097168 | tf_op jit(solution)/shard_map/all_gather | solution.py:29
  34.2 2.2 fusion
  36.5 72.7 %all-gather.13.cloned.1.call-done = bf16[2,2048,512]{2,1,0:T(8,128)(2,1)} async-done(((bf16[2,256,512]{2,1,0:T(8,128)(2,1)}), bf16[2,2048,512]{2,1,0:T(8,128)(2,1)}) %all-gather.13.cloned.1.call-update) | async-done | bytes 4194320 | tf_op jit(solution)/shard_map/all_gather | solution.py:18
  109.2 2.9 fusion.9
  112.1 70.6 %all-gather.11.cloned.1.call-done = bf16[2,2048,512]{2,1,0:T(8,128)(2,1)} async-done(((bf16[2,256,512]{2,1,0:T(8,128)(2,1)}), bf16[2,2048,512]{2,1,0:T(8,128)(2,1)}) %all-gather.11.cloned.1.call-update) | async-done | bytes 4194320 | tf_op jit(solution)/shard_map/all_gather | solution.py:19
  182.7 2.9 fusion.18
  185.6 2.5 collective-permute-start
  188.1 1.3 collective-permute-done
  189.6 66.6 %all-gather.9.cloned.1.call-done = bf16[2,2048,512]{2,1,0:T(8,128)(2,1)} async-done(((bf16[2,256,512]{2,1,0:T(8,128)(2,1)}), bf16[2,2048,512]{2,1,0:T(8,128)(2,1)}) %all-gather.9.cloned.1.call-update) | async-done | bytes 4194320 | tf_op jit(solution)/shard_map/all_gather | solution.py:20
  256.1 75.1 %all-gather.15.cloned.1.call-done = bf16[2,512,2048]{2,1,0:T(8,128)(2,1)} async-done(((bf16[2,512,256]{2,1,0:T(8,128)(2,1)}), bf16[2,512,2048]{2,1,0:T(8,128)(2,1)}) %all-gather.15.cloned.1.call-update) | async-done | bytes 4194320 | tf_op jit(solution)/shard_map/all_gather | solution.py:22
  331.2 6.1 %convolution_convert_fusion.1 = bf16[512,2048]{1,0:T(8,128)(2,1)} fusion(bf16[2,512,2048]{2,1,0:T(8,128)(2,1)} %all-gather.15.cloned.1.call-done, bf16[2,2048,512]{2,1,0:T(8,128)(2,1)} %all-gather.9.cloned.1.call-done, f32[514,512]{1,0:T(8,128)S(1)} %maximum_convert_fusion, f32[512]{0:T(512)S(1)} %bitcast.61, f32[512]{0:T(512)S(1)} %bitcast.62, ...), kind=kOutput, calls=%fused_computation.11 | convolution fusion | flops 2154561536 | bytes 11550720 | tf_op jit(solution)/shard_map/dot_general | solution.py:47
  337.4 29.5 %reduce-scatter.3.cloned.1.call-done = bf16[512,512]{1,0:T(8,128)(2,1)} async-done(((bf16[512,2048]{1,0:T(8,128)(2,1)}), bf16[512,512]{1,0:T(8,128)(2,1)}) %reduce-scatter.3.cloned.1.call-update) | async-done | bytes 524304 | tf_op jit(solution)/shard_map/reduce_scatter | solution.py:50
  366.9 2.0 add_convert_fusion.1
  368.9 22.6 %all-gather.17.cloned.1.call-done = bf16[512,2048]{1,0:T(8,128)(2,1)} async-done(((bf16[512,512]{1,0:T(8,128)(2,1)}), bf16[512,2048]{1,0:T(8,128)(2,1)}) %all-gather.17.cloned.1.call-update) | async-done | bytes 2097168 | tf_op jit(solution)/shard_map/all_gather | solution.py:29
  391.6 2.2 fusion.3
  393.8 3.0 fusion.6
  396.9 1.3 fusion.16
  398.2 3.4 collective-permute-start.1
  401.6 1.3 collective-permute-done.1
  403.0 6.2 %convolution_convert_fusion = bf16[512,2048]{1,0:T(8,128)(2,1)} fusion(bf16[2,512,2048]{2,1,0:T(8,128)(2,1)} %all-gather.15.cloned.1.call-done, bf16[2,2048,512]{2,1,0:T(8,128)(2,1)} %all-gather.9.cloned.1.call-done, f32[514,512]{1,0:T(8,128)S(1)} %maximum_convert_fusion.1, f32[512]{0:T(512)S(1)} %bitcast.59, f32[512]{0:T(512)S(1)} %bitcast.60, ...), kind=kOutput, calls=%fused_computation.10 | convolution fusion | flops 2154561536 | bytes 11550720 | tf_op jit(solution)/shard_map/dot_general | solution.py:47
  409.2 32.1 %reduce-scatter.5.cloned.1.call-done = bf16[512,512]{1,0:T(8,128)(2,1)} async-done(((bf16[512,2048]{1,0:T(8,128)(2,1)}), bf16[512,512]{1,0:T(8,128)(2,1)}) %reduce-scatter.5.cloned.1.call-update) | async-done | bytes 524304 | tf_op jit(solution)/shard_map/reduce_scatter | solution.py:50
  441.4 2.0 add_convert_fusion
  (36 shorter events, 2.5 us)
Async XLA Ops:
  6.5 3.4 copy-start.4
  6.5 27.7 %all-gather.7.cloned.1.call-start = ((), (), s32[]{:S(2)}) async-start(), calls=%async_computation.2 | async-start | bytes 2621440 | tf_op jit(solution)/shard_map/all_gather | solution.py:29
  7.3 101.9 %all-gather.13.cloned.1.call-start = ((), (), s32[]{:S(2)}) async-start(), calls=%async_computation.5 | async-start | bytes 4718592 | tf_op jit(solution)/shard_map/all_gather | solution.py:18
  8.0 174.7 %all-gather.11.cloned.1.call-start = ((), (), s32[]{:S(2)}) async-start(), calls=%async_computation.4 | async-start | bytes 4718592 | tf_op jit(solution)/shard_map/all_gather | solution.py:19
  8.7 247.4 %all-gather.9.cloned.1.call-start = ((), (), s32[]{:S(2)}) async-start(), calls=%async_computation.3 | async-start | bytes 4718592 | tf_op jit(solution)/shard_map/all_gather | solution.py:20
  9.3 321.9 %all-gather.15.cloned.1.call-start = ((), (), s32[]{:S(2)}) async-start(), calls=%async_computation.6 | async-start | bytes 4718592 | tf_op jit(solution)/shard_map/all_gather | solution.py:22
  9.9 357.0 %reduce-scatter.3.cloned.1.call-start = ((), (), s32[]{:S(2)}) async-start(), calls=%async_computation.7 | async-start | bytes 2621440 | tf_op jit(solution)/shard_map/reduce_scatter | solution.py:50
  34.2 75.0 %copy-start.2 = (bf16[512,2048]{1,0:T(8,128)(2,1)S(1)}, bf16[512,2048]{1,0:T(8,128)(2,1)}, u32[]{:S(2)}) copy-start(bf16[512,2048]{1,0:T(8,128)(2,1)} %all-gather.7.cloned.1.call-done) | copy-start | bytes 6291460
  112.1 76.0 %copy-start.5 = (f32[2,3,512]{2,0,1:T(2,128)S(1)}, f32[2,3,512]{2,0,1:T(2,128)}, u32[]{:S(2)}) copy-start(f32[2,3,512]{2,0,1:T(2,128)} %param.12) | copy-start | bytes 36868
  185.6 3.8 collective-permute-start
  337.3 29.5 %copy-start.1 = (bf16[512,512]{1,0:T(8,128)(2,1)S(1)}, bf16[512,512]{1,0:T(8,128)(2,1)}, u32[]{:S(2)}) copy-start(bf16[512,512]{1,0:T(8,128)(2,1)} %param.7) | copy-start | bytes 1572868
  337.3 54.2 %all-gather.17.cloned.1.call-start = ((), (), s32[]{:S(2)}) async-start(), calls=%async_computation.8 | async-start | bytes 2621440 | tf_op jit(solution)/shard_map/all_gather | solution.py:29
  368.9 72.5 %reduce-scatter.5.cloned.1.call-start = ((), (), s32[]{:S(2)}) async-start(), calls=%async_computation.9 | async-start | bytes 2621440 | tf_op jit(solution)/shard_map/reduce_scatter | solution.py:50
  391.6 2.2 copy-start.3
  393.8 3.0 copy-start.6
  398.2 4.7 %collective-permute-start.1 = (bf16[2,512]{1,0:T(2,128)(2,1)S(1)}, bf16[2,512]{1,0:T(2,128)(2,1)S(1)}, u32[]{:S(2)}, u32[]{:S(2)}) collective-permute-start(bf16[2,512]{1,0:T(2,128)(2,1)S(1)} %slice.121), channel_id=1, source_target_pairs={{0,4},{4,8},{8,12},{12,16},{16,20},{20,24},{24,28},{1,5},{5,9},{9,... | collective-permute-start | bytes 6152 | tf_op jit(solution)/shard_map/ppermute | solution.py:13
  409.2 32.2 %copy-start = (bf16[512,512]{1,0:T(8,128)(2,1)S(1)}, bf16[512,512]{1,0:T(8,128)(2,1)}, u32[]{:S(2)}) copy-start(bf16[512,512]{1,0:T(8,128)(2,1)} %add_convert_fusion.1) | copy-start | bytes 1572868
Sparse Core Ops, SparseCore 0:
  8.9 25.2 all-gather.6
  36.4 72.7 all-gather.12
  111.4 71.2 all-gather.10
  184.8 71.2 all-gather.8
  258.0 73.1 all-gather.14
  337.5 29.3 reduce-scatter.2
  369.0 22.5 all-gather.16
  409.3 31.9 reduce-scatter.4
where the time goes:
time: 450 us
  waiting for transfers between devices  399 us (89%)
  matrix products  22.4 us (5%)
  between operations  13.6 us (3%)
  other arithmetic  8.7 us (2%)
  starting transfers between devices  6.12 us (1%)
    all_gather x1, waiting for transfers between devices, on_device(): gathered_out = lax.all_gather(w_output, 'sp', axis=2, tiled=True)  75.1 us
    all_gather x1, waiting for transfers between devices, on_device(): lax.all_gather(w_value, 'sp', axis=1, tiled=True)  72.7 us
    all_gather x1, waiting for transfers between devices, on_device(): lax.all_gather(w_inner, 'sp', axis=1, tiled=True)  70.6 us
    all_gather x1, waiting for transfers between devices, on_device(): lax.all_gather(w_outer, 'sp', axis=1, tiled=True)  66.6 us
    reduce_scatter x2, waiting for transfers between devices, on_device(): lax.psum_scatter(terms.astype(jnp.float32).astype(jnp.bfloat16), 'tp', sc...  61.6 us
    all_gather x2, waiting for transfers between devices, on_device(): full_rows = lax.all_gather(stream_now, 'tp', axis=1, tiled=True)  46.9 us
    dot_general x2, matrix products, on_device(): jnp.dot(gated, layer_output, preferred_element_type=jnp.float32)  12.3 us
  transfers between devices with their start and end apart: 10, of which 10 were waited for; matrix products, arithmetic and copies ran while one was open for 2% of the time, Pallas kernels for 0%

commit v1 on v0

--- a/solution.py
+++ b/solution.py
@@ -19,7 +19,12 @@
         lax.all_gather(w_inner, "sp", axis=1, tiled=True),
         lax.all_gather(w_outer, "sp", axis=1, tiled=True),
     )
-    gathered_out = lax.all_gather(w_output, "sp", axis=2, tiled=True)
+    ring = [w_output]
+    for hop in range(7):
+        ring.append(lax.ppermute(ring[-1], "sp", [(dev, (dev + 1) % 8) for dev in range(8)]))
+    gathered_out = jnp.roll(
+        jnp.concatenate(ring[::-1], axis=2), (lax.axis_index("sp") + 1) * ring[0].shape[2], axis=2
+    )
     stream_now = stream
     for layer_index in range(LAYERS):
         layer_value = gathered_in[0][layer_index]

time: 450 us -> 417 us (0.927)
  waiting for transfers between devices: 399 us -> 334 us
  local copies, waits for them, and re-layouts: 0.07 us -> 21.8 us
    ppermute x0 -> x7, waiting for transfers between devices: none -> 139 us  [on_device(): lax.ppermute(ring[-1], 'sp', [(dev, (dev + 1) % 8) for dev in range(8)])]
    all_gather x1 -> x0, waiting for transfers between devices: 75.1 us -> none  [on_device(): gathered_out = lax.all_gather(w_output, 'sp', axis=2, tiled=True)]
    all_gather x1, waiting for transfers between devices: 72.7 us -> 0.01 us  [on_device(): lax.all_gather(w_value, 'sp', axis=1, tiled=True)]
    all_gather x1, waiting for transfers between devices: 70.6 us -> 41 us  [on_device(): lax.all_gather(w_inner, 'sp', axis=1, tiled=True)]
    all_gather x2, waiting for transfers between devices: 46.9 us -> 22.7 us  [on_device(): full_rows = lax.all_gather(stream_now, 'tp', axis=1, tiled=True)]
    unnamed x14 -> x41, local copies, waits for them, and re-layouts: 0.03 us -> 19.3 us
  transfers between devices with their start and end apart: 10 -> 16, of which waited for: 10 -> 14; matrix products, arithmetic and copies ran while one was open for 2% -> 8% of each run, Pallas kernels for 0% -> 0%
where the time goes in v1:
time: 417 us; the launch traced here: 416 us
  waiting for transfers between devices  334 us (80%)
  matrix products  26.3 us (6%)
  local copies, waits for them, and re-layouts  21.8 us (5%)
  between operations  13.6 us (3%)
  other arithmetic  10.4 us (2%)
  starting transfers between devices  9.29 us (2%)
    ppermute x7, waiting for transfers between devices, on_device(): lax.ppermute(ring[-1], 'sp', [(dev, (dev + 1) % 8) for dev in range(8)])  139 us
    all_gather x1, waiting for transfers between devices, on_device(): lax.all_gather(w_outer, 'sp', axis=1, tiled=True)  65.3 us
    reduce_scatter x2, waiting for transfers between devices, on_device(): lax.psum_scatter(terms.astype(jnp.float32).astype(jnp.bfloat16), 'tp', sc...  62 us
    all_gather x1, waiting for transfers between devices, on_device(): lax.all_gather(w_inner, 'sp', axis=1, tiled=True)  41 us
    all_gather x2, waiting for transfers between devices, on_device(): full_rows = lax.all_gather(stream_now, 'tp', axis=1, tiled=True)  22.7 us
    unnamed x41, local copies, waits for them, and re-layouts  19.3 us
    dot_general x2, matrix products, on_device(): jnp.dot(gated, layer_output, preferred_element_type=jnp.float32)  14.3 us
  transfers between devices with their start and end apart: 16, of which 14 were waited for; matrix products, arithmetic and copies ran while one was open for 8% of the time, Pallas kernels for 0%

profile of v1, /device:TPU:0, one launch (start us, length us, event | category | flops | bytes accessed | tf_op | source)
XLA Modules:
  0.0 415.9 jit_solution(4566232432272280099)
XLA Ops:
  9.4 3.0 collective-permute-start.1
  12.4 15.2 %collective-permute-done.1 = bf16[2,512,256]{2,1,0:T(8,128)(2,1)S(1)} collective-permute-done((bf16[2,512,256]{2,1,0:T(8,128)(2,1)}, bf16[2,512,256]{2,1,0:T(8,128)(2,1)S(1)}, u32[]{:S(2)}, u32[]{:S(2)}) %collective-permute-start.1) | collective-permute-done | bytes 524320 | tf_op jit(solution)/shard_map/ppermute | solution.py:24
  27.6 15.8 %collective-permute-done.2 = bf16[2,512,256]{2,1,0:T(8,128)(2,1)S(1)} collective-permute-done((bf16[2,512,256]{2,1,0:T(8,128)(2,1)S(1)}, bf16[2,512,256]{2,1,0:T(8,128)(2,1)S(1)}, u32[]{:S(2)}, u32[]{:S(2)}) %collective-permute-start.2) | collective-permute-done | bytes 524320 | tf_op jit(solution)/shard_map/ppermute | solution.py:24
  43.3 26.3 %collective-permute-done.3 = bf16[2,512,256]{2,1,0:T(8,128)(2,1)S(1)} collective-permute-done((bf16[2,512,256]{2,1,0:T(8,128)(2,1)S(1)}, bf16[2,512,256]{2,1,0:T(8,128)(2,1)S(1)}, u32[]{:S(2)}, u32[]{:S(2)}) %collective-permute-start.3) | collective-permute-done | bytes 524320 | tf_op jit(solution)/shard_map/ppermute | solution.py:24
  69.7 16.8 %collective-permute-done.4 = bf16[2,512,256]{2,1,0:T(8,128)(2,1)S(1)} collective-permute-done((bf16[2,512,256]{2,1,0:T(8,128)(2,1)S(1)}, bf16[2,512,256]{2,1,0:T(8,128)(2,1)S(1)}, u32[]{:S(2)}, u32[]{:S(2)}) %collective-permute-start.4) | collective-permute-done | bytes 524320 | tf_op jit(solution)/shard_map/ppermute | solution.py:24
  86.5 27.5 %collective-permute-done.5 = bf16[2,512,256]{2,1,0:T(8,128)(2,1)S(1)} collective-permute-done((bf16[2,512,256]{2,1,0:T(8,128)(2,1)S(1)}, bf16[2,512,256]{2,1,0:T(8,128)(2,1)S(1)}, u32[]{:S(2)}, u32[]{:S(2)}) %collective-permute-start.5) | collective-permute-done | bytes 524320 | tf_op jit(solution)/shard_map/ppermute | solution.py:24
  114.7 26.5 %collective-permute-done.6 = bf16[2,512,256]{2,1,0:T(8,128)(2,1)} collective-permute-done((bf16[2,512,256]{2,1,0:T(8,128)(2,1)S(1)}, bf16[2,512,256]{2,1,0:T(8,128)(2,1)}, u32[]{:S(2)}, u32[]{:S(2)}) %collective-permute-start.6) | collective-permute-done | bytes 524320 | tf_op jit(solution)/shard_map/ppermute | solution.py:24
  142.1 2.1 fusion
  144.2 11.4 %collective-permute-done.7 = bf16[2,512,256]{2,1,0:T(8,128)(2,1)} collective-permute-done((bf16[2,512,256]{2,1,0:T(8,128)(2,1)}, bf16[2,512,256]{2,1,0:T(8,128)(2,1)}, u32[]{:S(2)}, u32[]{:S(2)}) %collective-permute-start.7) | collective-permute-done | bytes 524320 | tf_op jit(solution)/shard_map/ppermute | solution.py:24
  164.7 2.4 constant_dynamic-update-slice_fusion.7
  174.5 3.9 fusion.9
  178.4 41.0 %all-gather.10.cloned.1.call-done = bf16[2,2048,512]{2,1,0:T(8,128)(2,1)} async-done(((bf16[2,256,512]{2,1,0:T(8,128)(2,1)}), bf16[2,2048,512]{2,1,0:T(8,128)(2,1)}) %all-gather.10.cloned.1.call-update) | async-done | bytes 4194320 | tf_op jit(solution)/shard_map/all_gather | solution.py:19
  219.4 3.2 fusion.18
  222.5 2.5 collective-permute-start
  227.4 65.3 %all-gather.8.cloned.1.call-done = bf16[2,2048,512]{2,1,0:T(8,128)(2,1)} async-done(((bf16[2,256,512]{2,1,0:T(8,128)(2,1)}), bf16[2,2048,512]{2,1,0:T(8,128)(2,1)}) %all-gather.8.cloned.1.call-update) | async-done | bytes 4194320 | tf_op jit(solution)/shard_map/all_gather | solution.py:20
  292.7 7.2 %convolution_convert_fusion.1 = bf16[512,2048]{1,0:T(8,128)(2,1)} fusion(bf16[2,512,4096]{2,1,0:T(8,128)(2,1)} %constant_dynamic-update-slice_fusion, s32[]{:T(128)S(6)} %select_n.14, bf16[2,2048,512]{2,1,0:T(8,128)(2,1)} %all-gather.8.cloned.1.call-done, f32[514,512]{1,0:T(8,128)} %maximum_convert_fusion, f32[512]{0:T(512)S(1)} %bitcast.61, ...), kind=kOutput, calls=%fused_computation.11 | convolution fusion | flops 2154561536 | bytes 11550724 | tf_op jit(solution)/shard_map/dot_general | solution.py:52
  300.0 29.8 %reduce-scatter.3.cloned.1.call-done = bf16[512,512]{1,0:T(8,128)(2,1)} async-done(((bf16[512,2048]{1,0:T(8,128)(2,1)}), bf16[512,512]{1,0:T(8,128)(2,1)}) %reduce-scatter.3.cloned.1.call-update) | async-done | bytes 524304 | tf_op jit(solution)/shard_map/reduce_scatter | solution.py:55
  329.8 2.0 add_convert_fusion.1
  331.9 22.7 %all-gather.14.cloned.1.call-done = bf16[512,2048]{1,0:T(8,128)(2,1)} async-done(((bf16[512,512]{1,0:T(8,128)(2,1)}), bf16[512,2048]{1,0:T(8,128)(2,1)}) %all-gather.14.cloned.1.call-update) | async-done | bytes 2097168 | tf_op jit(solution)/shard_map/all_gather | solution.py:34
  354.5 2.1 fusion.3
  356.6 3.7 fusion.6
  362.0 3.6 collective-permute-start.8
  367.9 7.1 %convolution_convert_fusion = bf16[512,2048]{1,0:T(8,128)(2,1)} fusion(bf16[2,512,4096]{2,1,0:T(8,128)(2,1)} %constant_dynamic-update-slice_fusion, s32[]{:T(128)S(6)} %add.62, s32[]{:T(128)S(6)} %select_n.14, bf16[2,2048,512]{2,1,0:T(8,128)(2,1)} %all-gather.8.cloned.1.call-done, f32[514,512]{1,0:T(8,128)} %maximum_convert_fusion.1, f32[512]{0:T(512)S(1)} %bitcast.59, ...), kind=kOutput, calls=%fused_computation.10 | convolution fusion | flops 2154561536 | bytes 11550728 | tf_op jit(solution)/shard_map/dot_general | solution.py:52
  375.0 32.1 %reduce-scatter.5.cloned.1.call-done = bf16[512,512]{1,0:T(8,128)(2,1)} async-done(((bf16[512,2048]{1,0:T(8,128)(2,1)}), bf16[512,512]{1,0:T(8,128)(2,1)}) %reduce-scatter.5.cloned.1.call-update) | async-done | bytes 524304 | tf_op jit(solution)/shard_map/reduce_scatter | solution.py:55
  (75 shorter events, 29.5 us)
Async XLA Ops:
  6.5 135.5 %all-gather.6.cloned.1.call-start = ((), (), s32[]{:S(2)}) async-start(), calls=%async_computation.2 | async-start | bytes 2621440 | tf_op jit(solution)/shard_map/all_gather | solution.py:34
  7.3 167.2 %all-gather.12.cloned.1.call-start = ((), (), s32[]{:S(2)}) async-start(), calls=%async_computation.5 | async-start | bytes 4718592 | tf_op jit(solution)/shard_map/all_gather | solution.py:18
  8.0 211.4 %all-gather.10.cloned.1.call-start = ((), (), s32[]{:S(2)}) async-start(), calls=%async_computation.4 | async-start | bytes 4718592 | tf_op jit(solution)/shard_map/all_gather | solution.py:19
  8.7 284.0 %all-gather.8.cloned.1.call-start = ((), (), s32[]{:S(2)}) async-start(), calls=%async_computation.3 | async-start | bytes 4718592 | tf_op jit(solution)/shard_map/all_gather | solution.py:20
  9.3 320.5 %reduce-scatter.3.cloned.1.call-start = ((), (), s32[]{:S(2)}) async-start(), calls=%async_computation.6 | async-start | bytes 2621440 | tf_op jit(solution)/shard_map/reduce_scatter | solution.py:55
  9.4 18.2 %collective-permute-start.1 = (bf16[2,512,256]{2,1,0:T(8,128)(2,1)}, bf16[2,512,256]{2,1,0:T(8,128)(2,1)S(1)}, u32[]{:S(2)}, u32[]{:S(2)}) collective-permute-start(bf16[2,512,256]{2,1,0:T(8,128)(2,1)} %param.13), channel_id=1, source_target_pairs={{0,4},{4,8},{8,12},{12,16},{16,20},{20,24},{24,28},{28,0},{1,5},{5... | collective-permute-start | bytes 1572872 | tf_op jit(solution)/shard_map/ppermute | solution.py:24
  27.6 15.8 %collective-permute-start.2 = (bf16[2,512,256]{2,1,0:T(8,128)(2,1)S(1)}, bf16[2,512,256]{2,1,0:T(8,128)(2,1)S(1)}, u32[]{:S(2)}, u32[]{:S(2)}) collective-permute-start(bf16[2,512,256]{2,1,0:T(8,128)(2,1)S(1)} %collective-permute-done.1), channel_id=1, source_target_pairs={{0,4},{4,8},{8,12},{12,16},{16,20},{20,24},{24,28},{28,0},{1,5},{5... | collective-permute-start | bytes 1572872 | tf_op jit(solution)/shard_map/ppermute | solution.py:24
  43.3 119.5 %copy-start.5 = (bf16[2,512,256]{2,1,0:T(8,128)(2,1)}, bf16[2,512,256]{2,1,0:T(8,128)(2,1)S(1)}, u32[]{:S(2)}) copy-start(bf16[2,512,256]{2,1,0:T(8,128)(2,1)S(1)} %collective-permute-done.2) | copy-start | bytes 1572868
  43.3 26.3 %collective-permute-start.3 = (bf16[2,512,256]{2,1,0:T(8,128)(2,1)S(1)}, bf16[2,512,256]{2,1,0:T(8,128)(2,1)S(1)}, u32[]{:S(2)}, u32[]{:S(2)}) collective-permute-start(bf16[2,512,256]{2,1,0:T(8,128)(2,1)S(1)} %collective-permute-done.2), channel_id=1, source_target_pairs={{0,4},{4,8},{8,12},{12,16},{16,20},{20,24},{24,28},{28,0},{1,5},{5... | collective-permute-start | bytes 1572872 | tf_op jit(solution)/shard_map/ppermute | solution.py:24
  69.7 93.2 %copy-start.7 = (bf16[2,512,256]{2,1,0:T(8,128)(2,1)}, bf16[2,512,256]{2,1,0:T(8,128)(2,1)S(1)}, u32[]{:S(2)}) copy-start(bf16[2,512,256]{2,1,0:T(8,128)(2,1)S(1)} %collective-permute-done.3) | copy-start | bytes 1572868
  69.7 16.8 %collective-permute-start.4 = (bf16[2,512,256]{2,1,0:T(8,128)(2,1)S(1)}, bf16[2,512,256]{2,1,0:T(8,128)(2,1)S(1)}, u32[]{:S(2)}, u32[]{:S(2)}) collective-permute-start(bf16[2,512,256]{2,1,0:T(8,128)(2,1)S(1)} %collective-permute-done.3), channel_id=1, source_target_pairs={{0,4},{4,8},{8,12},{12,16},{16,20},{20,24},{24,28},{28,0},{1,5},{5... | collective-permute-start | bytes 1572872 | tf_op jit(solution)/shard_map/ppermute | solution.py:24
  86.4 76.4 %copy-start.9 = (bf16[2,512,256]{2,1,0:T(8,128)(2,1)}, bf16[2,512,256]{2,1,0:T(8,128)(2,1)S(1)}, u32[]{:S(2)}) copy-start(bf16[2,512,256]{2,1,0:T(8,128)(2,1)S(1)} %collective-permute-done.4) | copy-start | bytes 1572868
  86.5 27.5 %collective-permute-start.5 = (bf16[2,512,256]{2,1,0:T(8,128)(2,1)S(1)}, bf16[2,512,256]{2,1,0:T(8,128)(2,1)S(1)}, u32[]{:S(2)}, u32[]{:S(2)}) collective-permute-start(bf16[2,512,256]{2,1,0:T(8,128)(2,1)S(1)} %collective-permute-done.4), channel_id=1, source_target_pairs={{0,4},{4,8},{8,12},{12,16},{16,20},{20,24},{24,28},{28,0},{1,5},{5... | collective-permute-start | bytes 1572872 | tf_op jit(solution)/shard_map/ppermute | solution.py:24
  113.9 49.0 %copy-start.11 = (bf16[2,512,256]{2,1,0:T(8,128)(2,1)}, bf16[2,512,256]{2,1,0:T(8,128)(2,1)S(1)}, u32[]{:S(2)}) copy-start(bf16[2,512,256]{2,1,0:T(8,128)(2,1)S(1)} %collective-permute-done.5) | copy-start | bytes 1572868
  113.9 27.3 %collective-permute-start.6 = (bf16[2,512,256]{2,1,0:T(8,128)(2,1)S(1)}, bf16[2,512,256]{2,1,0:T(8,128)(2,1)}, u32[]{:S(2)}, u32[]{:S(2)}) collective-permute-start(bf16[2,512,256]{2,1,0:T(8,128)(2,1)S(1)} %collective-permute-done.5), channel_id=1, source_target_pairs={{0,4},{4,8},{8,12},{12,16},{16,20},{20,24},{24,28},{28,0},{1,5},{5... | collective-permute-start | bytes 1572872 | tf_op jit(solution)/shard_map/ppermute | solution.py:24
  141.2 14.3 %collective-permute-start.7 = (bf16[2,512,256]{2,1,0:T(8,128)(2,1)}, bf16[2,512,256]{2,1,0:T(8,128)(2,1)}, u32[]{:S(2)}, u32[]{:S(2)}) collective-permute-start(bf16[2,512,256]{2,1,0:T(8,128)(2,1)} %collective-permute-done.6), channel_id=1, source_target_pairs={{0,4},{4,8},{8,12},{12,16},{16,20},{20,24},{24,28},{28,0},{1,5},{5... | collective-permute-start | bytes 1572872 | tf_op jit(solution)/shard_map/ppermute | solution.py:24
  144.1 19.7 %copy-start.4 = (bf16[2,512,256]{2,1,0:T(8,128)(2,1)S(1)}, bf16[2,512,256]{2,1,0:T(8,128)(2,1)}, u32[]{:S(2)}) copy-start(bf16[2,512,256]{2,1,0:T(8,128)(2,1)} %param.13) | copy-start | bytes 1572868
  163.8 10.6 %copy-start.2 = (bf16[512,2048]{1,0:T(8,128)(2,1)S(1)}, bf16[512,2048]{1,0:T(8,128)(2,1)}, u32[]{:S(2)}) copy-start(bf16[512,2048]{1,0:T(8,128)(2,1)} %all-gather.6.cloned.1.call-done) | copy-start | bytes 6291460
  222.5 3.8 collective-permute-start
  292.7 37.1 %copy-start.1 = (bf16[512,512]{1,0:T(8,128)(2,1)S(1)}, bf16[512,512]{1,0:T(8,128)(2,1)}, u32[]{:S(2)}) copy-start(bf16[512,512]{1,0:T(8,128)(2,1)} %param.7) | copy-start | bytes 1572868
  300.0 54.6 %all-gather.14.cloned.1.call-start = ((), (), s32[]{:S(2)}) async-start(), calls=%async_computation.7 | async-start | bytes 2621440 | tf_op jit(solution)/shard_map/all_gather | solution.py:34
  331.8 75.3 %reduce-scatter.5.cloned.1.call-start = ((), (), s32[]{:S(2)}) async-start(), calls=%async_computation.8 | async-start | bytes 2621440 | tf_op jit(solution)/shard_map/reduce_scatter | solution.py:55
  362.0 4.7 %collective-permute-start.8 = (bf16[2,512]{1,0:T(2,128)(2,1)S(1)}, bf16[2,512]{1,0:T(2,128)(2,1)S(1)}, u32[]{:S(2)}, u32[]{:S(2)}) collective-permute-start(bf16[2,512]{1,0:T(2,128)(2,1)S(1)} %slice.120), channel_id=1, source_target_pairs={{0,4},{4,8},{8,12},{12,16},{16,20},{20,24},{24,28},{1,5},{5,9},{9,... | collective-permute-start | bytes 6152 | tf_op jit(solution)/shard_map/ppermute | solution.py:13
  367.9 39.3 %copy-start = (bf16[512,512]{1,0:T(8,128)(2,1)S(1)}, bf16[512,512]{1,0:T(8,128)(2,1)}, u32[]{:S(2)}) copy-start(bf16[512,512]{1,0:T(8,128)(2,1)} %add_convert_fusion.1) | copy-start | bytes 1572868
  (5 other events, 31.7 us)
Sparse Core Ops, SparseCore 0:
  8.9 25.2 all-gather.5
  36.4 99.5 all-gather.11
  138.1 81.1 all-gather.9
  221.4 71.2 all-gather.7
  300.1 29.7 reduce-scatter.2
  331.9 22.5 all-gather.13
  375.1 31.9 reduce-scatter.4
